TPU v7x, 32 devices: a whole 2x2x4 slice. The times are simulated.
32 devices in a mesh: sp: 8 (over z, y), dp: 4 (over x, core).
Axes of the slice: x: 2, y: 2, z: 4, core: 2. Of those that a mesh axis runs over, the one named last changes fastest.
Arguments:
- query: bfloat16 [4, 1536, 3072], P('dp', 'sp'), may hold values from -18 to 18
- latent: bfloat16 [4, 1536, 1024], P('dp', 'sp'), may hold values from -6 to 6
- rope_key: bfloat16 [4, 1536, 32], P('dp', 'sp'), may hold values from -5 to 5
- latent_norm_gain: float32 [1024], replicated, may hold values from 0.1 to 1.9
- key_up_matrix: bfloat16 [2048, 1024], P('dp'), may hold values from -0.1875 to 0.1875
- value_up_matrix: bfloat16 [2048, 1024], P('dp'), may hold values from -0.1875 to 0.1875
- out_grad: bfloat16 [4, 1536, 2048], P('dp', 'sp'), may hold values from -6 to 6
Outputs:
- query_grad: bfloat16 [4, 1536, 3072], P('dp', 'sp')
- latent_grad: float32 [4, 1536, 1024], P('dp', 'sp')
- rope_key_grad: float32 [4, 1536, 32], P('dp', 'sp')
- key_weight_grad: float32 [2048, 1024], P('dp')
- value_weight_grad: float32 [2048, 1024], P('dp')
- gain_grad: float32 [1024], replicated
All inputs are finite; a program needn't handle non-finite values.
Results may differ from a plain program's by a relative error of at most 0.011.
Values may be sent and summed in bfloat16 or wider, within the bound.
A program may use at most 256 MiB of HBM per device.

v0:
```python
import jax
import jax.numpy as jnp
from jax import lax
from jax.sharding import PartitionSpec as P

ATTENTION_HEADS = 32
PLAIN_HEAD_WIDTH = 64
ROPE = 32
VALUE_HEAD_WIDTH = 64
SPAN = 64
eps = 1e-06
rope_base = 10000.0


def rotate(values, cosine, sine):
    half = values.shape[-1] // 2
    first = values[..., :half]
    second = values[..., half:]
    return jnp.concatenate(
        [first * cosine - second * sine, second * cosine + first * sine], axis=-1
    )


def angles(length, width):
    inverse = 1.0 / rope_base ** (jnp.arange(0, width, 2, dtype=jnp.float32) / width)
    turned = jnp.arange(length, dtype=jnp.float32)[:, None] * inverse[None, :]
    return (jnp.cos(turned), jnp.sin(turned))


def attend_backward(arrived, rope_full):
    f32 = jnp.float32
    bf16 = jnp.bfloat16
    length = arrived.shape[0]
    local_heads = arrived.shape[1]
    width = PLAIN_HEAD_WIDTH + ROPE
    scale = width ** (-0.5)
    block = 512
    cosine, sine = angles(length, ROPE)
    neg = jnp.finfo(f32).min
    q_nope = arrived[:, :, :PLAIN_HEAD_WIDTH]
    q_rope = rotate(
        arrived[:, :, PLAIN_HEAD_WIDTH:width].astype(f32), cosine[:, None, :], sine[:, None, :]
    ).astype(bf16)
    key_nope = arrived[:, :, width : width + PLAIN_HEAD_WIDTH]
    values = arrived[:, :, width + PLAIN_HEAD_WIDTH : width + PLAIN_HEAD_WIDTH + VALUE_HEAD_WIDTH]
    d_out = arrived[:, :, width + PLAIN_HEAD_WIDTH + VALUE_HEAD_WIDTH :]
    k_rope = rotate(rope_full.astype(f32), cosine, sine).astype(bf16)
    dk_nope = jnp.zeros((length, local_heads, PLAIN_HEAD_WIDTH), f32)
    dk_rope = jnp.zeros((length, ROPE), f32)
    d_vals = jnp.zeros((length, local_heads, VALUE_HEAD_WIDTH), f32)
    dq_parts = []
    for begin in range(0, length, block):
        end = begin + block
        qn = q_nope[begin:end]
        qr = q_rope[begin:end]
        go = d_out[begin:end]
        scores = jnp.einsum("qhd,khd->hqk", qn, key_nope[:end], preferred_element_type=f32)
        scores = (
            scores + jnp.einsum("qhd,kd->hqk", qr, k_rope[:end], preferred_element_type=f32)
        ) * scale
        q_seg = jnp.arange(begin, end) // SPAN
        k_seg = jnp.arange(end) // SPAN
        allowed = k_seg[None, :] <= q_seg[:, None]
        scores = jnp.where(allowed[None], scores, neg)
        probs = jax.nn.softmax(scores, axis=-1)
        d_probs = jnp.einsum("qhd,khd->hqk", go, values[:end], preferred_element_type=f32)
        d_scores = probs * (d_probs - jnp.sum(probs * d_probs, axis=-1, keepdims=True))
        ds_b = d_scores.astype(bf16)
        p_b = probs.astype(bf16)
        dq_n = jnp.einsum("hqk,khd->qhd", ds_b, key_nope[:end], preferred_element_type=f32) * scale
        dq_r = jnp.einsum("hqk,kd->qhd", ds_b, k_rope[:end], preferred_element_type=f32) * scale
        dq_r = rotate(dq_r, cosine[begin:end, None, :], -sine[begin:end, None, :])
        dq_parts.append(jnp.concatenate([dq_n, dq_r], axis=-1).astype(bf16))
        dk_nope = dk_nope.at[:end].add(
            jnp.einsum("hqk,qhd->khd", ds_b, qn, preferred_element_type=f32) * scale
        )
        dk_rope = dk_rope.at[:end].add(
            jnp.einsum("hqk,qhd->kd", ds_b, qr, preferred_element_type=f32) * scale
        )
        d_vals = d_vals.at[:end].add(
            jnp.einsum("hqk,qhd->khd", p_b, go, preferred_element_type=f32)
        )
    query_part = jnp.concatenate(dq_parts, axis=0)
    grads = jnp.concatenate([query_part, dk_nope.astype(bf16), d_vals.astype(bf16)], axis=-1)
    return (grads, rotate(dk_rope, cosine, -sine))


def local(query, latent, rope_key, latent_norm_gain, key_up_matrix, value_up_matrix, out_grad):
    f32 = jnp.float32
    bf16 = jnp.bfloat16
    tokens = latent.shape[1]
    width = PLAIN_HEAD_WIDTH + ROPE
    head_cols = ATTENTION_HEADS * PLAIN_HEAD_WIDTH
    lat = latent[0].astype(f32)
    inv_rms = lax.rsqrt(jnp.mean(lat * lat, axis=-1, keepdims=True) + eps)
    normed = lat * inv_rms
    nlat = (normed * latent_norm_gain).astype(bf16)
    stacked = jnp.stack([key_up_matrix, value_up_matrix])
    whole = lax.all_gather(stacked, "dp", axis=1, tiled=True)
    kv_tok = jnp.einsum("tc,gnc->tgn", nlat, whole, preferred_element_type=f32).astype(bf16)
    heads_query = query[0].reshape(tokens, ATTENTION_HEADS, width)
    key_nope = kv_tok[:, 0].reshape(tokens, ATTENTION_HEADS, PLAIN_HEAD_WIDTH)
    values = kv_tok[:, 1].reshape(tokens, ATTENTION_HEADS, VALUE_HEAD_WIDTH)
    d_out = out_grad[0].reshape(tokens, ATTENTION_HEADS, VALUE_HEAD_WIDTH)
    packed = jnp.concatenate([heads_query, key_nope, values, d_out], axis=2)
    arrived = lax.all_to_all(packed, "sp", split_axis=1, concat_axis=0, tiled=True)
    rope_full = lax.all_gather(rope_key[0], "sp", axis=0, tiled=True)
    grads_heads, rope_full_grad = attend_backward(arrived, rope_full)
    returned = lax.all_to_all(grads_heads, "sp", split_axis=0, concat_axis=1, tiled=True)
    rope_grad = lax.psum_scatter(rope_full_grad, "sp", scatter_dimension=0, tiled=True)
    query_grad = returned[:, :, :width].reshape(tokens, ATTENTION_HEADS * width)
    key_cols = returned[:, :, width : width + PLAIN_HEAD_WIDTH].reshape(tokens, head_cols)
    value_cols = returned[:, :, width + PLAIN_HEAD_WIDTH :].reshape(tokens, head_cols)
    dkv = jnp.stack([key_cols, value_cols], axis=1)
    d_nlat = jnp.einsum("tgn,gnc->tc", dkv, whole, preferred_element_type=f32)
    latents_all = lax.all_gather(nlat[None], "dp", axis=0, tiled=True)
    columns = lax.all_to_all(dkv[None], "dp", split_axis=3, concat_axis=0, tiled=True)
    partial_value = jnp.einsum("stgr,stc->grc", columns, latents_all, preferred_element_type=f32)
    weight_grads = lax.psum(partial_value, "sp")
    gain_grad = lax.psum(jnp.sum(d_nlat * normed, axis=0), ("sp", "dp"))
    scaled = d_nlat * latent_norm_gain
    latent_grad = inv_rms * (scaled - normed * jnp.mean(scaled * normed, axis=-1, keepdims=True))
    return (
        query_grad[None],
        latent_grad[None],
        rope_grad[None],
        weight_grads[0],
        weight_grads[1],
        gain_grad,
    )


def solution(mesh):
    in_specs = (
        P("dp", "sp", None),
        P("dp", "sp", None),
        P("dp", "sp", None),
        P(),
        P("dp", None),
        P("dp", None),
        P("dp", "sp", None),
    )
    out_specs = (
        P("dp", "sp", None),
        P("dp", "sp", None),
        P("dp", "sp", None),
        P("dp", None),
        P("dp", None),
        P(),
    )
    return jax.shard_map(local, mesh=mesh, in_specs=in_specs, out_specs=out_specs, check_vma=False)
```

profile of v0, /device:TPU:0, one launch (start us, length us, event | category | flops | bytes accessed | tf_op | source)
XLA Modules:
  0.0 738.0 jit_solution(6265751976223707838)
XLA Ops:
  7.2 3.1 pad_maximum_fusion.2
  12.3 3.9 reshape_squeeze.12
  16.4 55.1 %all-gather.4.cloned.1.call-done = bf16[2,2048,1024]{2,1,0:T(8,128)(2,1)} async-done(((bf16[2,512,1024]{2,1,0:T(8,128)(2,1)}), bf16[2,2048,1024]{2,1,0:T(8,128)(2,1)}) %all-gather.4.cloned.1.call-update) | async-done | bytes 8388624 | tf_op jit(solution)/shard_map/all_gather | solution.py:99
  71.5 6.2 convolution_convert_fusion
  84.6 3.1 copy.95
  87.8 5.6 pad_maximum_fusion
  93.4 4.0 copy.97
  97.4 5.6 all-to-all-start
  103.2 126.8 %all-gather = bf16[1,1536,32]{2,0,1:T(2,128)(2,1)S(1)} all-gather(bf16[1,192,32]{2,0,1:T(2,128)(2,1)S(1)} %copy.99), channel_id=2, replica_groups=mesh['sp'=8,'dp'=4] {'sp'}, dimensions={1}, use_global_device_ids=true | all-gather | bytes 110592 | tf_op jit(solution)/shard_map/all_gather | solution.py:107
  236.4 8.3 %copy.98 = bf16[8,192,4,288]{1,0,3,2:T(8,128)(2,1)} copy(bf16[8,192,4,288]{3,1,2,0:T(8,128)(2,1)} %bitcast.8) | data formatting | bytes 7077888 | tf_op jit(solution)/shard_map/all_to_all | solution.py:106
  244.7 6.9 all_to_all.42
  254.7 3.3 fusion.152
  258.0 5.4 fusion.43
  263.4 3.1 multiply_reduce_fusion.2
  274.4 3.2 fusion.6
  280.8 2.8 multiply_reduce_fusion.1
  283.7 9.7 %multiply_convert_fusion.1 = bf16[4,512,1024]{2,1,0:T(8,128)(2,1)S(1)} fusion(f32[4,512,1024]{2,1,0:T(8,128)S(1)} %get-tuple-element.177, f32[4,512]{1,0:T(4,128)S(1)} %get-tuple-element.176, f32[4,512,1024]{2,1,0:T(8,128)S(1)} %get-tuple-element.171, f32[4,512]{1,0:T(4,128)S(1)} %get-tuple-element.170), kind=kLoop, calls=%fused_computation.12 | loop fusion | flops 8388608 | bytes 20987904 | tf_op jit(solution)/shard_map/convert_element_type | solution.py:68
  295.5 3.1 fusion.50
  300.5 8.5 %fusion.4 = f32[4,512,1536]{2,1,0:T(8,128)} fusion(f32[1536,512,4]{0,1,2:T(8,128)S(1)} %fusion.114, pred[512,1536]{1,0:T(8,128)(4,1)S(1)} %copy-done.13, bf16[1536,4,288]{0,2,1:T(8,128)(2,1)} %copy-done.3), kind=kOutput, calls=%fused_computation.5 | convolution fusion | flops 412090368 | bytes 27000832 | tf_op jit(solution)/shard_map/qhd,khd->hqk/dot_general | solution.py:57
  309.1 14.9 %fusion.154 = (f32[4,512]{1,0:T(4,128)S(1)}, f32[4,512,1536]{2,1,0:T(8,128)}) fusion(f32[4,512,1536]{2,1,0:T(8,128)} %fusion.4), kind=kOutput, calls=%fused_computation.226 | output fusion | flops 6292991 | bytes 25174016 | tf_op jit(solution)/shard_map/sub | solution.py:65
  323.9 11.8 %multiply_reduce_fusion = (f32[4,512]{1,0:T(4,128)S(1)}, f32[4,512,1536]{2,1,0:T(8,128)}) fusion(f32[4,512,1536]{2,1,0:T(8,128)} %get-tuple-element.173, f32[4,512]{1,0:T(4,128)S(1)} %get-tuple-element.172, bf16[1536,4,288]{0,2,1:T(8,128)(2,1)} %copy-done.3), kind=kOutput, calls=%fused_computation.7 | convolution fusion | flops 412088320 | bytes 26230784 | tf_op jit(solution)/shard_map/qhd,khd->hqk/dot_general | solution.py:66
  335.7 6.0 multiply_convert_fusion
  341.8 4.5 fusion.52
  346.3 2.7 fusion.53
  351.6 11.2 %fusion.37 = f32[1536,4,64]{0,2,1:T(8,128)} fusion(f32[1536,4,64]{0,2,1:T(8,128)} %scatter-add.24, bf16[1536,4,288]{0,2,1:T(8,128)(2,1)} %copy-done.3, f32[4,512]{1,0:T(4,128)S(1)} %get-tuple-element.170, f32[4,512,1024]{2,1,0:T(8,128)} %copy-done.2), kind=kOutput, calls=%fused_computation.53 | convolution fusion | flops 274992128 | bytes 19144704 | tf_op jit(solution)/shard_map/hqk,qhd->khd/dot_general | solution.py:81
  362.8 4.4 fusion.42
  367.2 13.7 %fusion.22 = bf16[1536,4,64]{0,2,1:T(8,128)(2,1)} fusion(f32[1536,4,64]{0,2,1:T(8,128)} %fusion.37, bf16[1536,4,288]{0,2,1:T(8,128)(2,1)} %copy-done.3, f32[4,512]{1,0:T(4,128)S(1)} %get-tuple-element.172, f32[4,512,1536]{2,1,0:T(8,128)} %fusion.4), kind=kOutput, calls=%fused_computation.36 | convolution fusion | flops 412880384 | bytes 27795456 | tf_op jit(solution)/shard_map/hqk,qhd->khd/dot_general | solution.py:81
  381.0 4.6 fusion.21
  385.9 3.0 pad_maximum_fusion.1
  388.8 5.8 copy.107
  394.6 4.6 all-to-all-start.1
  401.9 64.4 %all-to-all-done.1 = bf16[1536,4,224]{2,1,0:T(4,128)(2,1)} async-done(((bf16[1536,4,224]{2,1,0:T(4,128)(2,1)}), bf16[1536,4,224]{2,1,0:T(4,128)(2,1)}, u32[]{:S(2)}, u32[]{:S(2)}) %all-to-all-start.1) | async-done | bytes 2752544 | tf_op jit(solution)/shard_map/all_to_all | solution.py:109
  468.8 2.8 fusion.149
  471.5 2.6 copy.111
  481.1 2.7 fusion.60
  483.8 6.1 copy.116
  489.8 4.4 all-to-all-start.2
  494.3 3.7 fusion.58
  498.0 4.0 fusion.26
  503.7 16.3 %all-to-all-done.2 = bf16[1,192,2,2048]{1,2,0,3:T(2,128)(2,1)} async-done(((bf16[1,192,2,2048]{1,2,0,3:T(2,128)(2,1)}), bf16[1,192,2,2048]{1,2,0,3:T(2,128)(2,1)}, u32[]{:S(2)}, u32[]{:S(2)}) %all-to-all-start.2) | async-done | bytes 1572896 | tf_op jit(solution)/shard_map/all_to_all | solution.py:117
  520.0 6.0 copy.118
  526.0 5.7 convolution_bitcast_fusion.1
  531.7 34.6 %reduce-scatter.4.cloned.1.call-done = f32[192,32]{1,0:T(8,128)} async-done(((f32[1536,32]{1,0:T(8,128)}), f32[192,32]{1,0:T(8,128)}) %reduce-scatter.4.cloned.1.call-update) | async-done | bytes 24592
  569.2 3.0 broadcast_in_dim_reshape.3
  572.2 6.3 fusion.72
  578.5 44.0 %psum.15 = f32[1024]{0:T(1024)} all-reduce(f32[1024]{0:T(1024)S(1)} %get-tuple-element.138), channel_id=1, replica_groups=mesh['sp'=8,'dp'=4] {'sp','dp'}, use_global_device_ids=true, to_apply=%region_14.15 | all-reduce | flops 1024 | bytes 8192 | tf_op jit(solution)/shard_map/psum | solution.py:120
  623.6 102.6 %all-reduce.5.cloned.1.call-done = f32[2,512,1024]{2,1,0:T(8,128)} async-done(((f32[2,512,1024]{2,1,0:T(8,128)}), f32[2,512,1024]{2,1,0:T(8,128)}) %all-reduce.5.cloned.1.call-update) | async-done | bytes 4194320 | tf_op jit(solution)/shard_map/psum | solution.py:119
  726.2 4.8 slice_bitcast_fusion
  (168 shorter events, 54.3 us)
Async XLA Ops:
  7.2 3.2 copy-start.32
  7.2 64.3 %all-gather.4.cloned.1.call-start = ((), (), s32[]{:S(2)}) async-start(), calls=%async_computation.4 | async-start | bytes 10485760 | tf_op jit(solution)/shard_map/all_gather | solution.py:99
  10.3 5.9 copy-start.10
  10.4 61.1 %copy-start.41 = (f32[1024]{0:T(1024)S(1)}, f32[1024]{0:T(1024)}, u32[]{:S(2)}) copy-start(f32[1024]{0:T(1024)} %param.34) | copy-start | bytes 12292
  16.4 55.1 %copy-start.44 = (f32[192]{0:T(256)}, f32[192]{0:T(256)S(1)}, u32[]{:S(2)}) copy-start(f32[192]{0:T(256)S(1)} %add_rsqrt_fusion) | copy-start | bytes 2308
  97.4 5.7 copy-start.43
  97.4 139.0 %all-to-all-start = ((bf16[192,32,288]{2,0,1:T(8,128)(2,1)}), bf16[192,32,288]{2,0,1:T(8,128)(2,1)}, u32[]{:S(2)}, u32[]{:S(2)}) async-start(bf16[192,32,288]{2,0,1:T(8,128)(2,1)} %copy.97), calls=%async_computation | async-start | bytes 9437184 | tf_op jit(solution)/shard_map/all_to_all | solution.py:106
  251.6 11.8 %copy-start.3 = (bf16[1536,4,288]{0,2,1:T(8,128)(2,1)}, bf16[1536,4,288]{0,2,1:T(8,128)(2,1)S(1)}, u32[]{:S(2)}) copy-start(bf16[1536,4,288]{0,2,1:T(8,128)(2,1)S(1)} %all_to_all.42) | copy-start | bytes 10616836
  251.6 2.0 copy-start.16
  251.6 2.0 copy-start.18
  251.6 2.0 copy-start.24
  254.7 3.3 copy-start.5
  263.4 3.4 copy-start.4
  268.0 5.0 copy-start.7
  268.0 5.0 copy-start.9
  277.6 3.3 copy-start.2
  293.4 5.2 copy-start.1
  298.7 1.8 copy-start.13
  323.9 11.8 %slice-start = ((s8[12582912]{0:T(1024)(128)(4,1)}), s8[4194304]{0:T(1024)(128)(4,1)S(1)}, s32[]{:S(2)}) async-start(s8[12582912]{0:T(1024)(128)(4,1)} %bitcast.187), calls=%async_computation.8 | async-start | bytes 8388608
  323.9 11.8 %slice-start.1 = ((s8[12582912]{0:T(1024)(128)(4,1)}), s8[4194304]{0:T(1024)(128)(4,1)S(1)}, s32[]{:S(2)}) async-start(s8[12582912]{0:T(1024)(128)(4,1)} %bitcast.187), calls=%async_computation.9 | async-start | bytes 8388608
  323.9 11.8 %slice-start.2 = ((s8[12582912]{0:T(1024)(128)(4,1)}), s8[4194304]{0:T(1024)(128)(4,1)S(1)}, s32[]{:S(2)}) async-start(s8[12582912]{0:T(1024)(128)(4,1)} %bitcast.187), calls=%async_computation.10 | async-start | bytes 8388608
  341.8 7.1 copy-start
  346.3 2.7 copy-start.34
  380.9 4.7 copy-start.21
  380.9 4.8 copy-start.39
  380.9 4.8 copy-start.40
  380.9 4.8 copy-start.22
  380.9 4.8 copy-start.37
  380.9 4.8 copy-start.38
  380.9 4.9 copy-start.23
  380.9 4.9 copy-start.35
  380.9 4.9 copy-start.36
  380.9 4.9 copy-start.25
  381.0 4.9 copy-start.26
  381.0 4.9 copy-start.27
  381.0 4.9 copy-start.33
  394.6 4.9 copy-start.11
  394.6 4.9 copy-start.42
  394.6 4.9 copy-start.45
  394.6 71.6 %all-to-all-start.1 = ((bf16[1536,4,224]{2,1,0:T(4,128)(2,1)}), bf16[1536,4,224]{2,1,0:T(4,128)(2,1)}, u32[]{:S(2)}, u32[]{:S(2)}) async-start(bf16[1536,4,224]{2,1,0:T(4,128)(2,1)} %copy.107), calls=%async_computation.1 | async-start | bytes 6291456 | tf_op jit(solution)/shard_map/all_to_all | solution.py:109
  399.2 126.8 %all-gather.6.cloned.1.call-start = ((), (), s32[]{:S(2)}) async-start(), calls=%async_computation.5 | async-start | bytes 1966080 | tf_op jit(solution)/shard_map/all_gather | solution.py:116
  489.8 30.2 %all-to-all-start.2 = ((bf16[1,192,2,2048]{1,2,0,3:T(2,128)(2,1)}), bf16[1,192,2,2048]{1,2,0,3:T(2,128)(2,1)}, u32[]{:S(2)}, u32[]{:S(2)}) async-start(bf16[1,192,2,2048]{1,2,0,3:T(2,128)(2,1)} %copy.116), calls=%async_computation.2 | async-start | bytes 4194304 | tf_op jit(solution)/shard_map/all_to_all | solution.py:117
  494.3 72.0 %reduce-scatter.4.cloned.1.call-start = ((), (), s32[]{:S(2)}) async-start(), calls=%async_computation.7 | async-start | bytes 884736
  498.0 4.0 copy-start.47
  503.6 222.6 %all-reduce.5.cloned.1.call-start = ((), (), s32[]{:S(2)}) async-start(), calls=%async_computation.6 | async-start | bytes 8388608 | tf_op jit(solution)/shard_map/psum | solution.py:119
  567.9 4.3 copy-start.12
  568.2 4.0 copy-start.14
  568.2 4.0 copy-start.15
  (10 other events, 9.7 us)
Sparse Core Ops, SparseCore 0:
  10.5 60.9 all-gather.3
  401.6 19.9 all-gather.5
  503.8 62.4 reduce-scatter.3
  569.8 156.3 all-reduce.4
where the time goes:
time: 747 us; the launch traced here: 738 us
  waiting for transfers between devices  273 us (37%)
  blocking collectives  171 us (23%)
  matrix products  118 us (16%)
  local copies, waits for them, and re-layouts  87 us (12%)
  other arithmetic  59.6 us (8%)
  starting transfers between devices  15.1 us (2%)
  between operations  15 us (2%)
    all_gather x1, blocking collectives, local(): rope_full = lax.all_gather(rope_key[0], 'sp', axis=0, tiled=True)  127 us
    psum x1, waiting for transfers between devices, local(): weight_grads = lax.psum(partial_value, 'sp')  103 us
    all_to_all x1, waiting for transfers between devices, local(): lax.all_to_all(grads_heads, 'sp', split_axis=0, concat_axis=1, tiled=True)  64.4 us
    all_gather x1, waiting for transfers between devices, local(): whole = lax.all_gather(stacked, 'dp', axis=1, tiled=True)  55.1 us
    psum x1, blocking collectives, local(): gain_grad = lax.psum(jnp.sum(d_nlat * normed, axis=0), ('sp', 'dp'))  44 us
    unnamed x5, waiting for transfers between devices  34.6 us
    dot_general x3, matrix products, attend_backward(): jnp.einsum('hqk,qhd->khd', p_b, go, preferred_element_type=f32)  30.3 us
    sub x3, other arithmetic, attend_backward(): probs = jax.nn.softmax(scores, axis=-1)  20.1 us
  transfers between devices with their start and end apart: 7, of which 5 were waited for; matrix products, arithmetic and copies ran while one was open for 10% of the time, Pallas kernels for 0%

commit v1 on v0

--- a/solution.py
+++ b/solution.py
@@ -116,7 +116,11 @@
     latents_all = lax.all_gather(nlat[None], "dp", axis=0, tiled=True)
     columns = lax.all_to_all(dkv[None], "dp", split_axis=3, concat_axis=0, tiled=True)
     partial_value = jnp.einsum("stgr,stc->grc", columns, latents_all, preferred_element_type=f32)
-    weight_grads = lax.psum(partial_value, "sp")
+    weight_grads = partial_value
+    for hop in (1, 2, 4):
+        weight_grads = weight_grads + lax.ppermute(
+            weight_grads, "sp", [(dev, dev ^ hop) for dev in range(8)]
+        )
     gain_grad = lax.psum(jnp.sum(d_nlat * normed, axis=0), ("sp", "dp"))
     scaled = d_nlat * latent_norm_gain
     latent_grad = inv_rms * (scaled - normed * jnp.mean(scaled * normed, axis=-1, keepdims=True))

time: 747 us -> 1000 us (1.34)
  waiting for transfers between devices: 273 us -> 519 us
  blocking collectives: 171 us -> 197 us
    ppermute x0 -> x3, waiting for transfers between devices: none -> 182 us  [local(): lax.ppermute(weight_grads, 'sp', [(dev, dev ^ hop) for dev in range(8)])]
    unnamed x5 -> x4, waiting for transfers between devices: 34.6 us -> 216 us
    psum x1 -> x0, waiting for transfers between devices: 103 us -> none  [local(): weight_grads = lax.psum(partial_value, 'sp')]
    all_to_all x0 -> x1, blocking collectives: none -> 30.3 us  [local(): lax.all_to_all(dkv[None], 'dp', split_axis=3, concat_axis=0, tiled=True)]
    all_to_all x1 -> x0, waiting for transfers between devices: 16.3 us -> none  [local(): lax.all_to_all(dkv[None], 'dp', split_axis=3, concat_axis=0, tiled=True)]
  transfers between devices with their start and end apart: 7 -> 8, of which waited for: 5 -> 5; matrix products, arithmetic and copies ran while one was open for 10% -> 6% of each run, Pallas kernels for 0% -> 0%
where the time goes in v1:
time: 1000 us; the launch traced here: 994 us
  waiting for transfers between devices  519 us (52%)
  blocking collectives  197 us (20%)
  matrix products  109 us (11%)
  local copies, waits for them, and re-layouts  82 us (8%)
  other arithmetic  60.4 us (6%)
  between operations  15 us (2%)
  starting transfers between devices  11.7 us (1%)
    unnamed x4, waiting for transfers between devices  216 us
    ppermute x3, waiting for transfers between devices, local(): lax.ppermute(weight_grads, 'sp', [(dev, dev ^ hop) for dev in range(8)])  182 us
    all_gather x1, blocking collectives, local(): rope_full = lax.all_gather(rope_key[0], 'sp', axis=0, tiled=True)  127 us
    all_to_all x1, waiting for transfers between devices, local(): lax.all_to_all(grads_heads, 'sp', split_axis=0, concat_axis=1, tiled=True)  66 us
    all_gather x1, waiting for transfers between devices, local(): whole = lax.all_gather(stacked, 'dp', axis=1, tiled=True)  55.1 us
    psum x1, blocking collectives, local(): gain_grad = lax.psum(jnp.sum(d_nlat * normed, axis=0), ('sp', 'dp'))  40 us
    all_to_all x1, blocking collectives, local(): lax.all_to_all(dkv[None], 'dp', split_axis=3, concat_axis=0, tiled=True)  30.3 us
    dot_general x3, matrix products, attend_backward(): jnp.einsum('hqk,qhd->khd', p_b, go, preferred_element_type=f32)  30.3 us
  transfers between devices with their start and end apart: 8, of which 5 were waited for; matrix products, arithmetic and copies ran while one was open for 6% of the time, Pallas kernels for 0%

profile of v1, /device:TPU:0, one launch (start us, length us, event | category | flops | bytes accessed | tf_op | source)
XLA Modules:
  0.0 993.9 jit_solution(9897075457730060516)
XLA Ops:
  7.2 3.1 pad_maximum_fusion.2
  12.3 3.9 reshape_squeeze.12
  16.4 55.1 %all-gather.4.cloned.1.call-done = bf16[2,2048,1024]{2,1,0:T(8,128)(2,1)} async-done(((bf16[2,512,1024]{2,1,0:T(8,128)(2,1)}), bf16[2,2048,1024]{2,1,0:T(8,128)(2,1)}) %all-gather.4.cloned.1.call-update) | async-done | bytes 8388624 | tf_op jit(solution)/shard_map/all_gather | solution.py:99
  71.5 6.2 convolution_convert_fusion
  80.0 2.4 copy.94
  84.6 3.1 copy.95
  87.8 5.6 pad_maximum_fusion
  93.4 4.0 copy.97
  97.4 5.6 all-to-all-start
  103.1 126.8 %all-gather = bf16[1,1536,32]{2,0,1:T(2,128)(2,1)S(1)} all-gather(bf16[1,192,32]{2,0,1:T(2,128)(2,1)S(1)} %copy.99), channel_id=2, replica_groups=mesh['sp'=8,'dp'=4] {'sp'}, dimensions={1}, use_global_device_ids=true | all-gather | bytes 110592 | tf_op jit(solution)/shard_map/all_gather | solution.py:107
  236.3 8.3 copy.98
  244.6 6.9 all_to_all.42
  254.6 3.3 fusion.152
  257.9 5.4 fusion.43
  263.3 3.1 multiply_reduce_fusion.2
  274.3 3.2 fusion.6
  280.8 2.8 multiply_reduce_fusion.1
  287.5 3.1 fusion.50
  292.5 8.6 fusion.4
  301.1 14.9 %fusion.154 = (f32[4,512]{1,0:T(4,128)S(1)}, f32[4,512,1536]{2,1,0:T(8,128)}) fusion(f32[4,512,1536]{2,1,0:T(8,128)} %fusion.4), kind=kOutput, calls=%fused_computation.226 | output fusion | flops 6292991 | bytes 25174016 | tf_op jit(solution)/shard_map/sub | solution.py:65
  316.0 11.8 %multiply_reduce_fusion = (f32[4,512]{1,0:T(4,128)S(1)}, f32[4,512,1536]{2,1,0:T(8,128)}) fusion(f32[4,512,1536]{2,1,0:T(8,128)} %get-tuple-element.173, f32[4,512]{1,0:T(4,128)S(1)} %get-tuple-element.172, bf16[1536,4,288]{0,2,1:T(8,128)(2,1)} %copy-done.4), kind=kOutput, calls=%fused_computation.7 | convolution fusion | flops 412088320 | bytes 26230784 | tf_op jit(solution)/shard_map/qhd,khd->hqk/dot_general | solution.py:66
  327.8 6.0 multiply_convert_fusion
  333.8 4.5 fusion.52
  338.3 2.6 fusion.53
  343.6 11.2 %fusion.37 = f32[1536,4,64]{0,2,1:T(8,128)} fusion(f32[1536,4,64]{0,2,1:T(8,128)} %scatter-add.24, bf16[1536,4,288]{0,2,1:T(8,128)(2,1)} %copy-done.4, f32[4,512]{1,0:T(4,128)S(1)} %get-tuple-element.170, f32[4,512,1024]{2,1,0:T(8,128)} %copy-done.3), kind=kOutput, calls=%fused_computation.53 | convolution fusion | flops 274992128 | bytes 19144704 | tf_op jit(solution)/shard_map/hqk,qhd->khd/dot_general | solution.py:81
  354.8 4.4 fusion.42
  359.2 13.7 %fusion.22 = bf16[1536,4,64]{0,2,1:T(8,128)(2,1)} fusion(f32[1536,4,64]{0,2,1:T(8,128)} %fusion.37, bf16[1536,4,288]{0,2,1:T(8,128)(2,1)} %copy-done.4, f32[4,512]{1,0:T(4,128)S(1)} %get-tuple-element.172, f32[4,512,1536]{2,1,0:T(8,128)} %fusion.4), kind=kOutput, calls=%fused_computation.36 | convolution fusion | flops 412880384 | bytes 27795456 | tf_op jit(solution)/shard_map/hqk,qhd->khd/dot_general | solution.py:81
  373.0 4.6 fusion.21
  377.9 3.0 pad_maximum_fusion.1
  380.9 5.8 copy.107
  386.7 4.6 all-to-all-start.1
  392.4 66.0 %all-to-all-done.1 = bf16[1536,4,224]{2,1,0:T(4,128)(2,1)} async-done(((bf16[1536,4,224]{2,1,0:T(4,128)(2,1)}), bf16[1536,4,224]{2,1,0:T(4,128)(2,1)}, u32[]{:S(2)}, u32[]{:S(2)}) %all-to-all-start.1) | async-done | bytes 2752544 | tf_op jit(solution)/shard_map/all_to_all | solution.py:109
  458.4 2.3 copy.108
  462.6 2.7 fusion.149
  471.5 2.7 fusion.60
  474.2 6.1 copy.116
  480.2 30.3 %all_to_all.54 = bf16[1,192,2,2048]{1,2,0,3:T(2,128)(2,1)} all-to-all(bf16[1,192,2,2048]{1,2,0,3:T(2,128)(2,1)} %copy.116), channel_id=1, replica_groups=mesh['sp'=8,'dp'=4] {'dp'}, dimensions={3} | all-to-all | bytes 3145728 | tf_op jit(solution)/shard_map/all_to_all | solution.py:117
  510.6 6.0 copy.118
  516.6 3.7 convolution_bitcast_fusion.1
  521.6 90.7 %collective-permute-done = f32[2,512,1024]{2,1,0:T(8,128)S(1)} collective-permute-done((f32[2,512,1024]{2,1,0:T(8,128)S(1)}, f32[2,512,1024]{2,1,0:T(8,128)S(1)}, u32[]{:S(2)}, u32[]{:S(2)}) %collective-permute-start) | collective-permute-done | bytes 4194336 | tf_op jit(solution)/shard_map/ppermute | solution.py:121
  613.8 91.1 %collective-permute-done.1 = f32[2,512,1024]{2,1,0:T(8,128)S(1)} collective-permute-done((f32[2,512,1024]{2,1,0:T(8,128)S(1)}, f32[2,512,1024]{2,1,0:T(8,128)S(1)}, u32[]{:S(2)}, u32[]{:S(2)}) %collective-permute-start.1) | collective-permute-done | bytes 4194336 | tf_op jit(solution)/shard_map/ppermute | solution.py:121
  704.9 2.9 add.194
  712.3 215.7 %reduce-scatter.4.cloned.1.call-done = f32[192,32]{1,0:T(8,128)} async-done(((f32[1536,32]{1,0:T(8,128)}), f32[192,32]{1,0:T(8,128)}) %reduce-scatter.4.cloned.1.call-update) | async-done | bytes 24592
  930.9 3.0 broadcast_in_dim_reshape.3
  933.9 5.3 fusion.72
  939.2 40.0 %psum.7 = f32[1024]{0:T(1024)} all-reduce(f32[1024]{0:T(1024)S(1)} %get-tuple-element.138), channel_id=1, replica_groups=mesh['sp'=8,'dp'=4] {'sp','dp'}, use_global_device_ids=true, to_apply=%region_13.14 | all-reduce | flops 1024 | bytes 8192 | tf_op jit(solution)/shard_map/psum | solution.py:124
  980.3 4.4 add.195
  984.7 2.3 slice_bitcast_fusion
  (184 shorter events, 56.1 us)
Async XLA Ops:
  7.2 3.2 copy-start.35
  7.2 64.3 %all-gather.4.cloned.1.call-start = ((), (), s32[]{:S(2)}) async-start(), calls=%async_computation.4 | async-start | bytes 10485760 | tf_op jit(solution)/shard_map/all_gather | solution.py:99
  10.3 5.9 copy-start.13
  10.4 61.1 %copy-start.44 = (f32[1024]{0:T(1024)S(1)}, f32[1024]{0:T(1024)}, u32[]{:S(2)}) copy-start(f32[1024]{0:T(1024)} %param.34) | copy-start | bytes 12292
  16.4 55.1 %copy-start.47 = (f32[192]{0:T(256)}, f32[192]{0:T(256)S(1)}, u32[]{:S(2)}) copy-start(f32[192]{0:T(256)S(1)} %add_rsqrt_fusion) | copy-start | bytes 2308
  97.4 5.7 copy-start.46
  97.4 139.0 %all-to-all-start = ((bf16[192,32,288]{2,0,1:T(8,128)(2,1)}), bf16[192,32,288]{2,0,1:T(8,128)(2,1)}, u32[]{:S(2)}, u32[]{:S(2)}) async-start(bf16[192,32,288]{2,0,1:T(8,128)(2,1)} %copy.97), calls=%async_computation | async-start | bytes 9437184 | tf_op jit(solution)/shard_map/all_to_all | solution.py:106
  251.5 11.8 %copy-start.4 = (bf16[1536,4,288]{0,2,1:T(8,128)(2,1)}, bf16[1536,4,288]{0,2,1:T(8,128)(2,1)S(1)}, u32[]{:S(2)}) copy-start(bf16[1536,4,288]{0,2,1:T(8,128)(2,1)S(1)} %all_to_all.42) | copy-start | bytes 10616836
  254.5 3.3 copy-start.8
  263.3 3.4 copy-start.7
  267.9 5.0 copy-start.10
  267.9 5.0 copy-start.12
  277.5 3.3 copy-start.3
  285.5 5.2 copy-start.1
  316.0 11.8 %slice-start.2 = ((s8[12582912]{0:T(1024)(128)(4,1)}), s8[4194304]{0:T(1024)(128)(4,1)S(1)}, s32[]{:S(2)}) async-start(s8[12582912]{0:T(1024)(128)(4,1)} %bitcast.189), calls=%async_computation.9 | async-start | bytes 8388608
  316.0 11.8 %slice-start.3 = ((s8[12582912]{0:T(1024)(128)(4,1)}), s8[4194304]{0:T(1024)(128)(4,1)S(1)}, s32[]{:S(2)}) async-start(s8[12582912]{0:T(1024)(128)(4,1)} %bitcast.189), calls=%async_computation.10 | async-start | bytes 8388608
  316.0 11.8 %slice-start.4 = ((s8[12582912]{0:T(1024)(128)(4,1)}), s8[4194304]{0:T(1024)(128)(4,1)S(1)}, s32[]{:S(2)}) async-start(s8[12582912]{0:T(1024)(128)(4,1)} %bitcast.189), calls=%async_computation.11 | async-start | bytes 8388608
  333.8 7.1 copy-start
  338.3 2.7 copy-start.37
  372.9 4.7 copy-start.24
  372.9 4.8 copy-start.42
  372.9 4.8 copy-start.43
  372.9 4.8 copy-start.25
  372.9 4.8 copy-start.40
  372.9 4.8 copy-start.41
  372.9 4.9 copy-start.26
  373.0 4.9 copy-start.38
  373.0 4.9 copy-start.39
  373.0 4.9 copy-start.28
  373.0 4.9 copy-start.29
  373.0 4.9 copy-start.30
  373.0 4.9 copy-start.36
  386.7 4.6 copy-start.14
  386.7 4.7 copy-start.45
  386.7 4.7 copy-start.48
  386.7 71.7 %all-to-all-start.1 = ((bf16[1536,4,224]{2,1,0:T(4,128)(2,1)}), bf16[1536,4,224]{2,1,0:T(4,128)(2,1)}, u32[]{:S(2)}, u32[]{:S(2)}) async-start(bf16[1536,4,224]{2,1,0:T(4,128)(2,1)} %copy.107), calls=%async_computation.1 | async-start | bytes 6291456 | tf_op jit(solution)/shard_map/all_to_all | solution.py:109
  391.3 125.3 %all-gather.6.cloned.1.call-start = ((), (), s32[]{:S(2)}) async-start(), calls=%async_computation.5 | async-start | bytes 1966080 | tf_op jit(solution)/shard_map/all_gather | solution.py:116
  392.3 535.7 %reduce-scatter.4.cloned.1.call-start = ((), (), s32[]{:S(2)}) async-start(), calls=%async_computation.6 | async-start | bytes 884736
  520.3 92.0 %collective-permute-start = (f32[2,512,1024]{2,1,0:T(8,128)S(1)}, f32[2,512,1024]{2,1,0:T(8,128)S(1)}, u32[]{:S(2)}, u32[]{:S(2)}) collective-permute-start(f32[2,512,1024]{2,1,0:T(8,128)S(1)} %convolution_bitcast_fusion.1), channel_id=1, source_target_pairs={{0,4},{4,0},{8,12},{12,8},{16,20},{20,16},{24,28},{28,24},{1,5},{5... | collective-permute-start | bytes 12582920 | tf_op jit(solution)/shard_map/ppermute | solution.py:121
  612.3 97.1 %slice-start = ((s8[6291456]{0:T(1024)(128)(4,1)}), s8[4194304]{0:T(1024)(128)(4,1)S(1)}, s32[]{:S(2)}) async-start(s8[6291456]{0:T(1024)(128)(4,1)} %bitcast.187), calls=%async_computation.7 | async-start | bytes 8388608
  613.7 94.8 %copy-start.2 = (bf16[4,512,1024]{2,1,0:T(8,128)(2,1)S(1)}, bf16[4,512,1024]{2,1,0:T(8,128)(2,1)}, u32[]{:S(2)}) copy-start(bf16[4,512,1024]{2,1,0:T(8,128)(2,1)} %copy-done.1) | copy-start | bytes 12582916
  613.7 95.7 %slice-start.1 = ((s8[6291456]{0:T(1024)(128)(4,1)}), s8[2097152]{0:T(1024)(128)(4,1)S(1)}, s32[]{:S(2)}) async-start(s8[6291456]{0:T(1024)(128)(4,1)} %bitcast.187), calls=%async_computation.8 | async-start | bytes 4194304
  613.7 91.2 %collective-permute-start.1 = (f32[2,512,1024]{2,1,0:T(8,128)S(1)}, f32[2,512,1024]{2,1,0:T(8,128)S(1)}, u32[]{:S(2)}, u32[]{:S(2)}) collective-permute-start(f32[2,512,1024]{2,1,0:T(8,128)S(1)} %add.193), channel_id=1, source_target_pairs={{0,8},{4,12},{8,0},{12,4},{16,24},{20,28},{24,16},{28,20},{1,9},{5... | collective-permute-start | bytes 12582920 | tf_op jit(solution)/shard_map/ppermute | solution.py:121
  707.8 272.5 %collective-permute-start.2 = (f32[2,512,1024]{2,1,0:T(8,128)}, f32[2,512,1024]{2,1,0:T(8,128)}, u32[]{:S(2)}, u32[]{:S(2)}) collective-permute-start(f32[2,512,1024]{2,1,0:T(8,128)} %add.194), channel_id=1, source_target_pairs={{0,16},{4,20},{8,24},{12,28},{16,0},{20,4},{24,8},{28,12},{1,17},{... | collective-permute-start | bytes 12582920 | tf_op jit(solution)/shard_map/ppermute | solution.py:121
  709.4 220.1 %copy-start.6 = (bf16[192,8,4,224]{3,0,2,1:T(8,128)(2,1)S(1)}, bf16[192,8,4,224]{3,0,2,1:T(8,128)(2,1)}, u32[]{:S(2)}) copy-start(bf16[192,8,4,224]{3,0,2,1:T(8,128)(2,1)} %copy-done.5) | copy-start | bytes 8257540
  929.6 4.3 copy-start.15
  929.9 4.0 copy-start.17
  929.9 4.0 copy-start.18
  (16 other events, 20.3 us)
Sparse Core Ops, SparseCore 0:
  10.5 60.9 all-gather.3
  394.3 19.9 all-gather.5
  712.4 215.5 reduce-scatter.3
